TPU v7x, 32 devices: a whole 2x2x4 slice. The times are simulated.
32 devices in a mesh: sp: 4 (over y, x), tp: 8 (over z, core).
Axes of the slice: x: 2, y: 2, z: 4, core: 2. Of those that a mesh axis runs over, the one named last changes fastest.
Arguments:
- queries: bfloat16 [1536, 2048], P('sp', 'tp'), may hold values from -6 to 6
- keys: bfloat16 [1536, 2048], P('sp', 'tp'), may hold values from -6 to 6
- values: bfloat16 [1536, 2048], P('sp', 'tp'), may hold values from -6 to 6
- key_bias: bfloat16 [1536, 32], P('sp', 'tp'), may hold values from -16 to 0
- head_gain: float32 [32, 64], P('tp'), may hold values from 0.1 to 1.9
- out_weight: bfloat16 [2048, 2048], P('tp'), may hold values from -0.125 to 0.125
- residual: bfloat16 [1536, 2048], P(('sp', 'tp')), may hold values from -6 to 6
- norm_gain: float32 [2048], replicated, may hold values from 0.1 to 1.9
- gate_proj: bfloat16 [4, 2048, 7168], P('sp', None, 'tp'), may hold values from -0.125 to 0.125
- up_proj: bfloat16 [4, 2048, 7168], P('sp', None, 'tp'), may hold values from -0.125 to 0.125
- down_proj: bfloat16 [4, 7168, 2048], P('sp', 'tp'), may hold values from -0.0625 to 0.0625
- expert_choice: int32 [1536, 2], P(('sp', 'tp')), may hold values from 0 to 3, all different within a row; in each aligned block of 48 rows (0 to 47, 48 to 95, ...) at most 48 rows name the same one
- expert_weights: float32 [1536, 2], P(('sp', 'tp')), may hold values from 0.2 to 1
Outputs:
- layer_out: bfloat16 [1536, 2048], P(('sp', 'tp'))
Inputs may be any that keep to these rules, and one draw needn't show every extreme that they name: `expert_choice`: in each aligned block of 48 rows (the rows of one device), no expert is named more than 48 times; the two experts of a row differ.
All inputs are finite; a program needn't handle non-finite values.
Results may differ from a plain program's by a relative error of at most 0.019.
Values may be sent and summed in bfloat16 or wider, within the bound.
A program may use at most 128 MiB of HBM per device.

v0:
```python
import jax
import jax.numpy as jnp
from jax import lax
from jax.sharding import PartitionSpec as P

epsilon = 1e-06


def rms_scaled(values_in):
    return values_in * lax.rsqrt(jnp.mean(values_in * values_in, axis=-1, keepdims=True) + epsilon)


def expert_partial(row_block, gate_matrix, up_matrix, down_matrix):
    gate_part = jnp.dot(row_block, gate_matrix, preferred_element_type=jnp.float32)
    up_part = jnp.dot(row_block, up_matrix, preferred_element_type=jnp.float32)
    hidden = (jax.nn.silu(gate_part) * up_part).astype(jnp.bfloat16)
    return jnp.dot(hidden, down_matrix, preferred_element_type=jnp.float32)


def choice_ranks(routes, experts_all):
    flat_routes = routes.reshape(routes.shape[:-2] + (-1,))
    onehot = (flat_routes[..., None] == jnp.arange(experts_all, dtype=jnp.int32)).astype(jnp.int32)
    before = jnp.cumsum(onehot, axis=-2) - onehot
    return jnp.sum(before * onehot, axis=-1).reshape(routes.shape)


def slot_tokens(slot_index, targets, missing):
    flat_slots = slot_index.reshape(-1)
    owners = jnp.arange(flat_slots.shape[0], dtype=jnp.int32) // 2
    matches = flat_slots[None, :] == jnp.arange(targets, dtype=jnp.int32)[:, None]
    owner_found = jnp.sum(jnp.where(matches, owners[None, :], 0), axis=1)
    return jnp.where(jnp.any(matches, axis=1), owner_found, missing)


def on_device(
    queries,
    keys,
    values,
    key_bias,
    head_gain,
    out_weight,
    residual,
    norm_gain,
    gate_proj,
    up_proj,
    down_proj,
    expert_choice,
    expert_weights,
):
    rows_own = queries.shape[0]
    heads_here = head_gain.shape[0]
    head_size = head_gain.shape[1]
    model_width = out_weight.shape[1]
    seq_devices = lax.axis_size("sp")
    head_devices = lax.axis_size("tp")
    own_start = lax.axis_index("sp") * rows_own
    query_pos = own_start + jnp.arange(rows_own, dtype=jnp.int32)
    query_heads = queries.reshape(rows_own, heads_here, head_size)

    def key_block(slot_state, key_rows, value_rows, bias_rows, key_start):
        key_heads = key_rows.reshape(rows_own, heads_here, head_size)
        value_heads = value_rows.reshape(rows_own, heads_here, head_size)
        scores = jnp.einsum(
            "qhd,khd->hqk", query_heads, key_heads, preferred_element_type=jnp.float32
        ) * head_size ** (-0.5)
        scores = scores + bias_rows.astype(jnp.float32).T[:, None, :]
        key_pos = key_start + jnp.arange(rows_own, dtype=jnp.int32)
        earlier = (key_pos[None, :] < query_pos[:, None])[None, :, :]
        log_drops = jnp.where(earlier, jax.nn.log_sigmoid(-scores), 0.0)
        suffix = lax.cumsum(log_drops, axis=2, reverse=True) - log_drops
        within = jnp.where(earlier, jnp.exp(jax.nn.log_sigmoid(scores) + suffix), 0.0).astype(
            jnp.bfloat16
        )
        block_part = jnp.einsum(
            "hqk,khd->qhd", within, value_heads, preferred_element_type=jnp.float32
        )
        block_index = key_start // rows_own
        sums_new = lax.dynamic_update_index_in_dim(
            slot_state[0], block_part.reshape(rows_own, heads_here * head_size), block_index, 0
        )
        totals_new = lax.dynamic_update_index_in_dim(
            slot_state[1], jnp.sum(log_drops, axis=2), block_index, 0
        )
        return (sums_new, totals_new)

    empty_state = (
        jnp.zeros((seq_devices, rows_own, heads_here * head_size), jnp.float32),
        jnp.zeros((seq_devices, heads_here, rows_own), jnp.float32),
    )
    key_piece = lax.all_gather(keys, "sp", axis=0, tiled=True)
    value_piece = lax.all_gather(values, "sp", axis=0, tiled=True)
    bias_piece = lax.all_gather(key_bias, "sp", axis=0, tiled=True)

    def visit(block_count, state_in):
        offset = block_count * rows_own

        def take_rows(array):
            return lax.dynamic_slice_in_dim(array, offset, rows_own, 0)

        def compute(state_now):
            return key_block(
                state_now,
                take_rows(key_piece),
                take_rows(value_piece),
                take_rows(bias_piece),
                offset,
            )

        def keep(state_now):
            return state_now

        return lax.cond(offset <= own_start, compute, keep, state_in)

    block_sums, totals = lax.fori_loop(0, key_piece.shape[0] // rows_own, visit, empty_state)
    carried = jnp.sum(totals, axis=0, keepdims=True) - jnp.cumsum(totals, axis=0)
    factors = jnp.exp(carried).transpose(0, 2, 1)[..., None]
    mixture = jnp.sum(
        factors * block_sums.reshape(seq_devices, rows_own, heads_here, head_size), axis=0
    )
    attended = (
        (rms_scaled(mixture) * head_gain)
        .astype(jnp.bfloat16)
        .reshape(rows_own, heads_here * head_size)
    )
    row_share = rows_own // head_devices
    merged = lax.all_to_all(attended, "tp", split_axis=0, concat_axis=1, tiled=True)
    projected = jnp.dot(
        merged,
        lax.all_gather(out_weight, "tp", axis=0, tiled=True),
        preferred_element_type=jnp.float32,
    )
    stream = (residual.astype(jnp.float32) + projected).astype(jnp.bfloat16)
    normed = (rms_scaled(stream.astype(jnp.float32)) * norm_gain).astype(jnp.bfloat16)
    local_experts = gate_proj.shape[0]
    experts_all = local_experts * seq_devices
    capacity = 4 * rows_own // (head_devices * experts_all)
    own_slots = expert_choice * capacity + choice_ranks(expert_choice, experts_all)
    wanted = slot_tokens(own_slots, experts_all * capacity, row_share)
    outgoing = jnp.take(normed, wanted, axis=0, mode="fill", fill_value=0)
    arrived = lax.all_to_all(
        outgoing.reshape(seq_devices, local_experts, capacity, model_width),
        "sp",
        split_axis=0,
        concat_axis=0,
        tiled=True,
    )
    row_piece = lax.all_gather(arrived, "tp", axis=0, tiled=True)
    count_rows = row_piece.shape[0]
    partials = jnp.stack(
        [
            expert_partial(
                row_piece[:, 0].reshape(-1, model_width), gate_proj[0], up_proj[0], down_proj[0]
            ).reshape(count_rows, capacity, model_width)
        ],
        axis=1,
    )
    summed = lax.psum_scatter(partials.astype(jnp.bfloat16), "tp", scatter_dimension=0, tiled=True)
    returned = lax.all_to_all(summed, "sp", split_axis=0, concat_axis=0, tiled=True).reshape(
        experts_all * capacity, model_width
    )
    picked = jnp.take(returned, own_slots, axis=0).astype(jnp.float32)
    combined = jnp.sum(expert_weights[:, :, None] * picked, axis=1)
    return (stream.astype(jnp.float32) + combined).astype(jnp.bfloat16)


def solution(mesh):
    placed = (
        P("sp", "tp"),
        P("sp", "tp"),
        P("sp", "tp"),
        P("sp", "tp"),
        P("tp", None),
        P("tp", None),
        P(("sp", "tp"), None),
        P(),
        P("sp", None, "tp"),
        P("sp", None, "tp"),
        P("sp", "tp", None),
        P(("sp", "tp"), None),
        P(("sp", "tp"), None),
    )
    return jax.shard_map(
        on_device, mesh=mesh, in_specs=placed, out_specs=P(("sp", "tp"), None), check_vma=False
    )
```

profile of v0, /device:TPU:0, one launch (start us, length us, event | category | flops | bytes accessed | tf_op | source)
XLA Modules:
  0.0 380.5 jit_solution(13210839301603181166)
XLA Ops:
  6.5 0.7 all-gather.3.cloned.1.call-update
  7.3 1.1 copy.81
  8.4 1.1 copy.82
  9.4 1.7 copy.83
  11.2 11.0 %all_gather.17 = bf16[1536,4]{0,1:T(4,128)(2,1)} all-gather(bf16[384,4]{0,1:T(4,128)(2,1)} %param.20), channel_id=1, replica_groups=mesh['sp'=4,'tp'=8] {'sp'}, dimensions={0}, use_global_device_ids=true | all-gather | bytes 15360 | tf_op jit(solution)/shard_map/all_gather | solution.py:92
  22.2 12.4 %all_gather.15 = bf16[1536,256]{0,1:T(8,128)(2,1)} all-gather(bf16[384,256]{0,1:T(8,128)(2,1)S(1)} %copy.81), channel_id=1, replica_groups=mesh['sp'=4,'tp'=8] {'sp'}, dimensions={0}, use_global_device_ids=true | all-gather | bytes 983040 | tf_op jit(solution)/shard_map/all_gather | solution.py:91
  34.5 13.4 %all_gather.16 = bf16[1536,256]{0,1:T(8,128)(2,1)} all-gather(bf16[384,256]{0,1:T(8,128)(2,1)S(1)} %copy.82), channel_id=1, replica_groups=mesh['sp'=4,'tp'=8] {'sp'}, dimensions={0}, use_global_device_ids=true | all-gather | bytes 983040 | tf_op jit(solution)/shard_map/all_gather | solution.py:90
  47.9 1.3 broadcast_in_dim.84
  49.2 0.6 broadcast_in_dim.85
  49.8 28.2 %while.17 = (s32[]{:T(128)}, f32[4,384,256]{1,2,0:T(8,128)}, f32[4,4,384]{2,1,0:T(4,128)}, s32[]{:T(128)}, bf16[1536,256]{0,1:T(8,128)(2,1)}, /*index=5*/bf16[15...) while((s32[]{:T(128)}, f32[4,384,256]{1,2,0:T(8,128)}, ...), condition=%wide.region_6.7_spmd.clone.clone, body=%wide.region_0.6_spmd.clone.clone.sunk | while | flops 246117120 | bytes 38572464 | solution.py:114
  49.8 28.0 %conditional.4 = ((f32[4,384,256]{1,2,0:T(8,128)}, f32[4,4,384]{2,1,0:T(4,128)})) conditional(s32[]{:T(128)} %convert_element_type.76, (f32[4,384,256]{1,2,0:T(8,128)}, f32[4,4,384]{2,1,0:T(4,128)}) %tuple.53, (s32[]{:T(128)}, bf16[1536,256]{0,1:T(8,128)(2,1)}, s32[]{:T(128)}, bf16[1536,256]{0,1:T(8,128)(2,1)}, bf16[384,4,64]{0,2,1:T(8,128)(2,1)}, ...), branch_computations={%region_1.0_spmd, %region_2.5_spmd} | conditional | flops 246117120 | bytes 38570716 | solution.py:112
  49.8 1.1 constant_dynamic-slice_fusion
  50.8 0.7 convert_bitcast_fusion
  51.5 0.1 broadcast_compare_fusion
  51.7 4.3 %fusion.15 = (f32[4,384]{1,0:T(4,128)S(1)}, f32[4,384,384]{1,2,0:T(8,128)S(1)}, f32[4,384,384]{2,1,0:T(8,128)}) fusion(f32[4,384]{1,0:T(4,128)S(1)} %convert_bitcast_fusion, pred[384,384]{0,1:T(8,128)(4,1)S(1)} %broadcast_compare_fusion, bf16[384,4,64]{0,2,1:T(8,128)(2,1)S(1)} %bitcast.92, bf16[384,4,64]{0,2,1:T(8,128)(2,1)} %get-tuple-element.177), kind=kOutput, calls=%fused_computation.33 | convolution fusion | flops 81984000 | bytes 5271552 | tf_op jit(solution)/shard_map/while/body/eval_jaxpr/cond/branch_1_fun/qhd,khd->hqk/dot_general | solution.py:63
  56.0 14.0 %fusion.2 = f32[4,384,3,128]{1,2,3,0:T(4,128)S(1)} fusion(f32[4,384,3,128]{1,3,2,0:T(8,128)S(1)} %bitcast.88), kind=kOutput, calls=%fused_computation.5 | output fusion | flops 74907648 | bytes 4718592 | tf_op jit(solution)/shard_map/reduce-window
  70.1 0.5 broadcast_add_fusion
  70.6 0.2 copy.79
  70.9 1.5 copy-done
  72.3 3.6 fusion.8
  76.0 0.3 fusion.27
  76.3 0.8 constant_dynamic-update-slice_fusion
  77.1 0.6 bitcast_dynamic-update-slice_fusion
  78.0 0.8 reduce_sum.74
  78.7 0.8 fusion.24
  79.5 1.6 fusion.22
  81.1 0.2 copy.84
  81.3 0.1 copy.85
  81.5 0.5 mul.104
  81.9 0.5 mul.105
  82.5 0.7 multiply_convert_fusion.2
  83.2 4.8 %all-to-all-start = ((bf16[8,48,256]{2,1,0:T(8,128)(2,1)}), bf16[8,48,256]{2,1,0:T(8,128)(2,1)S(1)}, u32[]{:S(2)}, u32[]{:S(2)}) async-start(bf16[8,48,256]{2,1,0:T(8,128)(2,1)} %multiply_convert_fusion.2), calls=%async_computation | async-start | bytes 393216 | tf_op jit(solution)/shard_map/all_to_all | solution.py:126
  88.1 0.1 copy.88
  88.2 0.1 eq.30
  88.3 0.1 fusion.26
  88.4 0.1 reduce_window_sum.40
  88.5 0.2 select_reduce_fusion.1
  88.7 0.1 reshape.172
  88.9 0.1 copy.91
  89.0 0.1 eq.34
  89.2 0.1 fusion.25
  89.3 0.1 select_reduce_fusion
  89.4 0.1 select_n.105
  89.5 6.8 %all-to-all-done = bf16[8,48,256]{2,1,0:T(8,128)(2,1)S(1)} async-done(((bf16[8,48,256]{2,1,0:T(8,128)(2,1)}), bf16[8,48,256]{2,1,0:T(8,128)(2,1)S(1)}, u32[]{:S(2)}, u32[]{:S(2)}) %all-to-all-start) | async-done | bytes 196640 | tf_op jit(solution)/shard_map/all_to_all | solution.py:126
  96.4 5.1 %multiply_reduce_fusion.1 = (f32[48]{0:T(128)S(1)}, f32[48,2048]{1,0:T(8,128)S(1)}) fusion(bf16[48,2048]{1,0:T(8,128)(2,1)S(1)} %bitcast.94, bf16[2048,2048]{1,0:T(8,128)(2,1)} %all-gather.3.cloned.1.call-done, bf16[48,2048]{1,0:T(8,128)(2,1)S(1)} %copy-done.1), kind=kOutput, calls=%fused_computation.54 | convolution fusion | flops 403242944 | bytes 9175232 | tf_op jit(solution)/shard_map/dot_general | solution.py:127
  101.5 0.1 multiply_convert_fusion.1
  101.6 1.1 gather_fusion
  102.8 0.1 broadcast_select_fusion
  102.9 96.4 %all_to_all.26 = bf16[4,1,48,2048]{3,2,1,0:T(8,128)(2,1)} all-to-all(bf16[4,1,48,2048]{3,2,1,0:T(8,128)(2,1)S(1)} %broadcast_select_fusion), channel_id=1, replica_groups=mesh['sp'=4,'tp'=8] {'sp'}, dimensions={0} | all-to-all | bytes 1572864 | tf_op jit(solution)/shard_map/all_to_all | solution.py:140
  199.4 63.5 %all-gather.5.cloned.1.call-done = bf16[32,1,48,2048]{3,2,1,0:T(8,128)(2,1)} async-done(((bf16[4,1,48,2048]{3,2,1,0:T(8,128)(2,1)}), bf16[32,1,48,2048]{3,2,1,0:T(8,128)(2,1)}) %all-gather.5.cloned.1.call-update) | async-done | bytes 6291472 | tf_op jit(solution)/shard_map/all_gather | solution.py:147
  262.9 10.0 %fusion.18 = f32[1536,896]{1,0:T(8,128)S(1)} fusion(bf16[1536,2048]{1,0:T(8,128)(2,1)} %bitcast.101, bf16[1,2048,896]{2,1,0:T(8,128)(2,1)} %param.25), kind=kOutput, calls=%fused_computation.38 | convolution fusion | flops 5637144576 | bytes 15466496 | tf_op jit(solution)/shard_map/dot_general | solution.py:14
  272.9 7.1 %multiply_convert_fusion = bf16[1536,896]{1,0:T(8,128)(2,1)S(1)} fusion(f32[1536,896]{1,0:T(8,128)S(1)} %fusion.18, bf16[1536,2048]{1,0:T(8,128)(2,1)S(1)} %bitcast.102, bf16[1,2048,896]{2,1,0:T(8,128)(2,1)S(1)} %copy-done.7), kind=kOutput, calls=%fused_computation.35 | convolution fusion | flops 5645402112 | bytes 18219008 | tf_op jit(solution)/shard_map/dot_general | solution.py:15
  280.0 8.7 %convert_bitcast_fusion.1 = bf16[32,1,48,2048]{3,2,0,1:T(8,128)(2,1)} fusion(bf16[32,48,896]{2,1,0:T(8,128)(2,1)S(1)} %bitcast.103, bf16[1,896,2048]{2,1,0:T(8,128)(2,1)S(1)} %copy-done.8), kind=kOutput, calls=%fused_computation.34 | convolution fusion | flops 5640290304 | bytes 12713984 | tf_op jit(solution)/shard_map/dot_general | solution.py:17
  288.8 68.5 %reduce-scatter.2.cloned.1.call-done = bf16[4,1,48,2048]{3,2,0,1:T(8,128)(2,1)} async-done(((bf16[32,1,48,2048]{3,2,0,1:T(8,128)(2,1)}), bf16[4,1,48,2048]{3,2,0,1:T(8,128)(2,1)}) %reduce-scatter.2.cloned.1.call-update) | async-done | bytes 786448 | tf_op jit(solution)/shard_map/reduce_scatter | solution.py:157
  357.3 3.7 all-to-all-start.2
  361.1 0.1 copy.94
  361.2 0.1 reshape.184
  361.3 0.1 copy.90
  361.4 0.1 copy.87
  361.5 8.6 %all-to-all-done.2 = bf16[4,1,48,2048]{3,2,1,0:T(8,128)(2,1)S(1)} async-done(((bf16[4,1,48,2048]{3,2,1,0:T(8,128)(2,1)}), bf16[4,1,48,2048]{3,2,1,0:T(8,128)(2,1)S(1)}, u32[]{:S(2)}, u32[]{:S(2)}) %all-to-all-start.2) | async-done | bytes 786464 | tf_op jit(solution)/shard_map/all_to_all | solution.py:158
  370.1 0.8 gather_fusion.1
  370.9 0.3 reshape.183
  371.2 2.1 multiply_reduce_fusion
  373.3 0.7 add_convert_fusion
  (48 shorter events, 0.6 us)
Async XLA Ops:
  6.5 89.9 %all-gather.3.cloned.1.call-start = ((), (), s32[]{:S(2)}) async-start(), calls=%async_computation.4 | async-start | bytes 9437184 | tf_op jit(solution)/shard_map/all_gather | solution.py:129
  70.6 1.7 copy-start
  79.5 2.9 copy-start.4
  81.1 7.0 %copy-start.3 = (s32[48,2]{0,1:T(2,128)S(1)}, s32[48,2]{0,1:T(2,128)}, u32[]{:S(2)}) copy-start(s32[48,2]{0,1:T(2,128)} %param.28) | copy-start | bytes 1156
  81.3 15.1 %copy-start.1 = (bf16[48,2048]{1,0:T(8,128)(2,1)S(1)}, bf16[48,2048]{1,0:T(8,128)(2,1)}, u32[]{:S(2)}) copy-start(bf16[48,2048]{1,0:T(8,128)(2,1)} %param.23) | copy-start | bytes 589828
  83.2 13.1 %all-to-all-start = ((bf16[8,48,256]{2,1,0:T(8,128)(2,1)}), bf16[8,48,256]{2,1,0:T(8,128)(2,1)S(1)}, u32[]{:S(2)}, u32[]{:S(2)}) async-start(bf16[8,48,256]{2,1,0:T(8,128)(2,1)} %multiply_convert_fusion.2), calls=%async_computation | async-start | bytes 393216 | tf_op jit(solution)/shard_map/all_to_all | solution.py:126
  88.0 174.9 %all-gather.5.cloned.1.call-start = ((), (), s32[]{:S(2)}) async-start(), calls=%async_computation.5 | async-start | bytes 7077888 | tf_op jit(solution)/shard_map/all_gather | solution.py:147
  96.4 5.1 %copy-start.2 = (f32[2048]{0:T(1024)S(1)}, f32[2048]{0:T(1024)}, u32[]{:S(2)}) copy-start(f32[2048]{0:T(1024)} %param.24) | copy-start | bytes 24580
  199.3 158.0 %reduce-scatter.2.cloned.1.call-start = ((), (), s32[]{:S(2)}) async-start(), calls=%async_computation.6 | async-start | bytes 7077888 | tf_op jit(solution)/shard_map/reduce_scatter | solution.py:157
  262.9 10.0 %copy-start.6 = (bf16[32,1,48,2048]{3,2,1,0:T(8,128)(2,1)S(1)}, bf16[32,1,48,2048]{3,2,1,0:T(8,128)(2,1)}, u32[]{:S(2)}) copy-start(bf16[32,1,48,2048]{3,2,1,0:T(8,128)(2,1)} %all-gather.5.cloned.1.call-done) | copy-start | bytes 18874372
  262.9 10.0 %copy-start.7 = (bf16[1,2048,896]{2,1,0:T(8,128)(2,1)S(1)}, bf16[1,2048,896]{2,1,0:T(8,128)(2,1)}, u32[]{:S(2)}) copy-start(bf16[1,2048,896]{2,1,0:T(8,128)(2,1)} %param.26) | copy-start | bytes 11010052
  272.9 7.1 %copy-start.8 = (bf16[1,896,2048]{2,1,0:T(8,128)(2,1)S(1)}, bf16[1,896,2048]{2,1,0:T(8,128)(2,1)}, u32[]{:S(2)}) copy-start(bf16[1,896,2048]{2,1,0:T(8,128)(2,1)} %param.27) | copy-start | bytes 11010052
  288.8 72.6 %copy-start.5 = (f32[48,2]{0,1:T(2,128)S(1)}, f32[48,2]{0,1:T(2,128)}, u32[]{:S(2)}) copy-start(f32[48,2]{0,1:T(2,128)} %param.29) | copy-start | bytes 1156
  357.3 12.7 %all-to-all-start.2 = ((bf16[4,1,48,2048]{3,2,1,0:T(8,128)(2,1)}), bf16[4,1,48,2048]{3,2,1,0:T(8,128)(2,1)S(1)}, u32[]{:S(2)}, u32[]{:S(2)}) async-start(bf16[4,1,48,2048]{3,2,1,0:T(8,128)(2,1)} %bitcast.96), calls=%async_computation.3 | async-start | bytes 1572864 | tf_op jit(solution)/shard_map/all_to_all | solution.py:158
Sparse Core Ops, SparseCore 0:
  8.9 84.8 all-gather.2
  199.4 63.4 all-gather.4
  288.9 68.3 reduce-scatter.1
where the time goes:
time: 382 us; the launch traced here: 380 us
  waiting for transfers between devices  148 us (39%)
  blocking collectives  133 us (35%)
  matrix products  35.5 us (9%)
  other arithmetic  26.7 us (7%)
  local copies, waits for them, and re-layouts  14.7 us (4%)
  between operations  13.4 us (4%)
  starting transfers between devices  8.62 us (2%)
    all_to_all x1, blocking collectives, on_device(): lax.all_to_all(outgoing.reshape(seq_devices, local_experts, capacity, mod...  96.4 us
    reduce_scatter x1, waiting for transfers between devices, on_device(): lax.psum_scatter(partials.astype(jnp.bfloat16), 'tp', scatter_dimension=0...  68.5 us
    all_gather x1, waiting for transfers between devices, on_device(): row_piece = lax.all_gather(arrived, 'tp', axis=0, tiled=True)  63.5 us
    another operation x2, other arithmetic  14.1 us
    all_gather x1, blocking collectives, on_device(): key_piece = lax.all_gather(keys, 'sp', axis=0, tiled=True)  13.4 us
    all_gather x1, blocking collectives, on_device(): value_piece = lax.all_gather(values, 'sp', axis=0, tiled=True)  12.4 us
    all_gather x1, blocking collectives, on_device(): bias_piece = lax.all_gather(key_bias, 'sp', axis=0, tiled=True)  11 us
    dot_general x1, matrix products, expert_partial(): jnp.dot(row_block, gate_matrix, preferred_element_type=jnp.float32)  9.96 us
  transfers between devices with their start and end apart: 5, of which 4 were waited for; matrix products, arithmetic and copies ran while one was open for 10% of the time, Pallas kernels for 0%

commit v1 on v0

--- a/solution.py
+++ b/solution.py
@@ -4,6 +4,28 @@
 from jax.sharding import PartitionSpec as P
 
 epsilon = 1e-06
+
+
+def cut_along(x, dim, size):
+    before, after = (x.shape[:dim], x.shape[dim + 1 :])
+    return jnp.moveaxis(x.reshape(*before, size, -1, *after), dim, 0)
+
+
+def laid_out(blocks, dim):
+    dims = list(blocks.shape[1:])
+    dims[dim] *= blocks.shape[0]
+    return jnp.moveaxis(blocks, 0, dim).reshape(dims)
+
+
+def rotated_exchange(shard, axis, split_dim, concat_dim):
+    peers, index = (lax.axis_size(axis), lax.axis_index(axis))
+    pieces = cut_along(shard, split_dim, peers)
+    outs = [pieces[index]]
+    for turn in range(1, peers):
+        sent = pieces[(index + turn) % peers]
+        outs.append(lax.ppermute(sent, axis, [(i, (i + turn) % peers) for i in range(peers)]))
+    pieces = jnp.stack(outs)[(index - jnp.arange(peers)) % peers]
+    return laid_out(pieces, concat_dim)
 
 
 def rms_scaled(values_in):
@@ -137,12 +159,8 @@
     own_slots = expert_choice * capacity + choice_ranks(expert_choice, experts_all)
     wanted = slot_tokens(own_slots, experts_all * capacity, row_share)
     outgoing = jnp.take(normed, wanted, axis=0, mode="fill", fill_value=0)
-    arrived = lax.all_to_all(
-        outgoing.reshape(seq_devices, local_experts, capacity, model_width),
-        "sp",
-        split_axis=0,
-        concat_axis=0,
-        tiled=True,
+    arrived = rotated_exchange(
+        outgoing.reshape(seq_devices, local_experts, capacity, model_width), "sp", 0, 0
     )
     row_piece = lax.all_gather(arrived, "tp", axis=0, tiled=True)
     count_rows = row_piece.shape[0]

time: 382 us -> 390 us (1.021)
  blocking collectives: 133 us -> 36.7 us
  starting transfers between devices: 8.62 us -> 94.3 us
  waiting for transfers between devices: 148 us -> 157 us
  loops' own time: 0.31 us -> 8.81 us
    all_to_all x1 -> x0, blocking collectives: 96.4 us -> none  [on_device(): lax.all_to_all(outgoing.reshape(seq_devices, local_experts, capacity, mod...]
    ppermute x0 -> x3, starting transfers between devices: none -> 85.6 us  [rotated_exchange(): lax.ppermute(sent, axis, [(i, (i + turn) % peers) for i in range(peers)])]
    another operation x1, loops' own time: 0.2 us -> 8.7 us  [on_device(): lax.fori_loop(0, key_piece.shape[0] // rows_own, visit, empty_state)]
    ppermute x0 -> x3, waiting for transfers between devices: none -> 7.42 us  [rotated_exchange(): lax.ppermute(sent, axis, [(i, (i + turn) % peers) for i in range(peers)])]
    another operation x2 -> x3, other arithmetic: 14.1 us -> 14.2 us
  transfers between devices with their start and end apart: 5 -> 8, of which waited for: 4 -> 6; matrix products, arithmetic and copies ran while one was open for 10% -> 10% of each run, Pallas kernels for 0% -> 0%
where the time goes in v1:
time: 390 us; the launch traced here: 389 us
  waiting for transfers between devices  157 us (40%)
  starting transfers between devices  94.3 us (24%)
  blocking collectives  36.7 us (9%)
  matrix products  35.5 us (9%)
  other arithmetic  26.8 us (7%)
  local copies, waits for them, and re-layouts  16.3 us (4%)
  between operations  13.8 us (4%)
  loops' own time  8.81 us (2%)
    ppermute x3, starting transfers between devices, rotated_exchange(): lax.ppermute(sent, axis, [(i, (i + turn) % peers) for i in range(peers)])  85.6 us
    reduce_scatter x1, waiting for transfers between devices, on_device(): lax.psum_scatter(partials.astype(jnp.bfloat16), 'tp', scatter_dimension=0...  68.5 us
    all_gather x1, waiting for transfers between devices, on_device(): row_piece = lax.all_gather(arrived, 'tp', axis=0, tiled=True)  64.4 us
    another operation x2, other arithmetic  14.1 us
    all_gather x1, blocking collectives, on_device(): key_piece = lax.all_gather(keys, 'sp', axis=0, tiled=True)  13.4 us
    all_gather x1, blocking collectives, on_device(): value_piece = lax.all_gather(values, 'sp', axis=0, tiled=True)  12.4 us
    all_gather x1, blocking collectives, on_device(): bias_piece = lax.all_gather(key_bias, 'sp', axis=0, tiled=True)  11 us
    dot_general x1, matrix products, expert_partial(): jnp.dot(row_block, gate_matrix, preferred_element_type=jnp.float32)  9.96 us
  transfers between devices with their start and end apart: 8, of which 6 were waited for; matrix products, arithmetic and copies ran while one was open for 10% of the time, Pallas kernels for 0%

profile of v1, /device:TPU:0, one launch (start us, length us, event | category | flops | bytes accessed | tf_op | source)
XLA Modules:
  0.0 388.6 jit_solution(7817281751383652254)
XLA Ops:
  6.5 0.7 all-gather.4.cloned.1.call-update
  7.3 1.1 copy.79
  8.4 1.1 copy.80
  9.4 1.7 copy.81
  11.2 11.0 %all_gather.17 = bf16[1536,4]{0,1:T(4,128)(2,1)} all-gather(bf16[384,4]{0,1:T(4,128)(2,1)} %param.20), channel_id=1, replica_groups=mesh['sp'=4,'tp'=8] {'sp'}, dimensions={0}, use_global_device_ids=true | all-gather | bytes 15360 | tf_op jit(solution)/shard_map/all_gather | solution.py:114
  22.2 12.4 %all_gather.15 = bf16[1536,256]{0,1:T(8,128)(2,1)} all-gather(bf16[384,256]{0,1:T(8,128)(2,1)S(1)} %copy.79), channel_id=1, replica_groups=mesh['sp'=4,'tp'=8] {'sp'}, dimensions={0}, use_global_device_ids=true | all-gather | bytes 983040 | tf_op jit(solution)/shard_map/all_gather | solution.py:113
  34.5 13.4 %all_gather.16 = bf16[1536,256]{0,1:T(8,128)(2,1)} all-gather(bf16[384,256]{0,1:T(8,128)(2,1)S(1)} %copy.80), channel_id=1, replica_groups=mesh['sp'=4,'tp'=8] {'sp'}, dimensions={0}, use_global_device_ids=true | all-gather | bytes 983040 | tf_op jit(solution)/shard_map/all_gather | solution.py:112
  47.9 1.3 broadcast_in_dim.85
  49.2 0.6 broadcast_in_dim.86
  49.8 36.7 %while.17 = (s32[]{:T(128)}, f32[4,384,256]{1,2,0:T(8,128)}, f32[4,4,384]{2,1,0:T(4,128)}, s32[]{:T(128)}, bf16[1536,256]{0,1:T(8,128)(2,1)}, /*index=5*/bf16[15...) while((s32[]{:T(128)}, f32[4,384,256]{1,2,0:T(8,128)}, ...), condition=%wide.region_6.7_spmd.clone.clone, body=%wide.region_0.6_spmd.clone.clone.sunk | while | flops 246117120 | bytes 38572464 | solution.py:136
  49.8 28.0 %conditional.4 = ((f32[4,384,256]{1,2,0:T(8,128)}, f32[4,4,384]{2,1,0:T(4,128)})) conditional(s32[]{:T(128)} %convert_element_type.76, (f32[4,384,256]{1,2,0:T(8,128)}, f32[4,4,384]{2,1,0:T(4,128)}) %tuple.56, (s32[]{:T(128)}, bf16[1536,256]{0,1:T(8,128)(2,1)}, s32[]{:T(128)}, bf16[1536,256]{0,1:T(8,128)(2,1)}, bf16[384,4,64]{0,2,1:T(8,128)(2,1)}, ...), branch_computations={%region_1.0_spmd, %region_2.5_spmd} | conditional | flops 246117120 | bytes 38570716 | solution.py:134
  49.8 1.1 constant_dynamic-slice_fusion
  50.8 0.7 convert_bitcast_fusion
  51.5 0.1 broadcast_compare_fusion
  51.7 4.3 %fusion.15 = (f32[4,384]{1,0:T(4,128)S(1)}, f32[4,384,384]{1,2,0:T(8,128)S(1)}, f32[4,384,384]{2,1,0:T(8,128)}) fusion(f32[4,384]{1,0:T(4,128)S(1)} %convert_bitcast_fusion, pred[384,384]{0,1:T(8,128)(4,1)S(1)} %broadcast_compare_fusion, bf16[384,4,64]{0,2,1:T(8,128)(2,1)S(1)} %bitcast.103, bf16[384,4,64]{0,2,1:T(8,128)(2,1)} %get-tuple-element.177), kind=kOutput, calls=%fused_computation.34 | convolution fusion | flops 81984000 | bytes 5271552 | tf_op jit(solution)/shard_map/while/body/eval_jaxpr/cond/branch_1_fun/qhd,khd->hqk/dot_general | solution.py:85
  56.0 14.0 %fusion.2 = f32[4,384,3,128]{1,2,3,0:T(4,128)S(1)} fusion(f32[4,384,3,128]{1,3,2,0:T(8,128)S(1)} %bitcast.99), kind=kOutput, calls=%fused_computation.6 | output fusion | flops 74907648 | bytes 4718592 | tf_op jit(solution)/shard_map/reduce-window
  70.1 0.5 broadcast_add_fusion
  70.6 0.2 copy.77
  70.9 1.5 copy-done
  72.3 3.6 fusion.8
  76.0 0.3 fusion.29
  76.3 0.8 constant_dynamic-update-slice_fusion
  77.1 0.6 bitcast_dynamic-update-slice_fusion
  86.5 0.8 reduce_sum.74
  87.2 0.8 fusion.24
  88.0 1.6 fusion.22
  89.6 0.2 copy.82
  89.9 0.1 copy.83
  90.0 0.5 mul.104
  90.5 0.5 mul.105
  91.0 0.7 multiply_convert_fusion.2
  91.8 4.8 %all-to-all-start = ((bf16[8,48,256]{2,1,0:T(8,128)(2,1)}), bf16[8,48,256]{2,1,0:T(8,128)(2,1)S(1)}, u32[]{:S(2)}, u32[]{:S(2)}) async-start(bf16[8,48,256]{2,1,0:T(8,128)(2,1)} %multiply_convert_fusion.2), calls=%async_computation | async-start | bytes 393216 | tf_op jit(solution)/shard_map/all_to_all | solution.py:148
  96.7 0.1 eq.36
  96.9 0.1 reduce_window_sum.40
  97.0 0.2 select_reduce_fusion.1
  97.2 0.1 reshape.223
  97.5 0.1 eq.40
  97.7 0.1 fusion.25
  97.8 0.1 select_reduce_fusion
  98.1 6.8 %all-to-all-done = bf16[8,48,256]{2,1,0:T(8,128)(2,1)S(1)} async-done(((bf16[8,48,256]{2,1,0:T(8,128)(2,1)}), bf16[8,48,256]{2,1,0:T(8,128)(2,1)S(1)}, u32[]{:S(2)}, u32[]{:S(2)}) %all-to-all-start) | async-done | bytes 196640 | tf_op jit(solution)/shard_map/all_to_all | solution.py:148
  104.9 5.1 %multiply_reduce_fusion.1 = (f32[48]{0:T(128)S(1)}, f32[48,2048]{1,0:T(8,128)S(1)}) fusion(bf16[48,2048]{1,0:T(8,128)(2,1)S(1)} %bitcast.105, bf16[2048,2048]{1,0:T(8,128)(2,1)} %all-gather.4.cloned.1.call-done, bf16[48,2048]{1,0:T(8,128)(2,1)S(1)} %copy-done.1), kind=kOutput, calls=%fused_computation.56 | convolution fusion | flops 403242944 | bytes 9175232 | tf_op jit(solution)/shard_map/dot_general | solution.py:149
  110.0 0.1 multiply_convert_fusion.1
  110.1 1.1 gather_fusion
  111.3 0.1 broadcast_select_fusion
  111.5 28.4 %collective-permute-start = (bf16[1,1,48,2048]{3,2,1,0:T(8,128)(2,1)S(1)}, bf16[1,1,48,2048]{3,2,1,0:T(8,128)(2,1)S(1)}, u32[]{:S(2)}, u32[]{:S(2)}) collective-permute-start(bf16[1,1,48,2048]{3,2,1,0:T(8,128)(2,1)S(1)} %get-tuple-element.272), channel_id=1, source_target_pairs={{0,8},{8,16},{16,24},{24,0},{1,9},{9,17},{17,25},{25,1},{2,10},{10... | collective-permute-start | bytes 589832 | tf_op jit(solution)/shard_map/ppermute | solution.py:26
  139.9 57.1 %collective-permute-start.1 = (bf16[1,1,48,2048]{3,2,1,0:T(8,128)(2,1)S(1)}, bf16[1,1,48,2048]{3,2,1,0:T(8,128)(2,1)S(1)}, u32[]{:S(2)}, u32[]{:S(2)}) collective-permute-start(bf16[1,1,48,2048]{3,2,1,0:T(8,128)(2,1)S(1)} %get-tuple-element.271), channel_id=1, source_target_pairs={{0,16},{8,24},{16,0},{24,8},{1,17},{9,25},{17,1},{25,9},{2,18},{10... | collective-permute-start | bytes 589832 | tf_op jit(solution)/shard_map/ppermute | solution.py:26
  197.1 5.2 %collective-permute-done = bf16[1,1,48,2048]{3,2,1,0:T(8,128)(2,1)S(1)} collective-permute-done((bf16[1,1,48,2048]{3,2,1,0:T(8,128)(2,1)S(1)}, bf16[1,1,48,2048]{3,2,1,0:T(8,128)(2,1)S(1)}, u32[]{:S(2)}, u32[]{:S(2)}) %collective-permute-start) | collective-permute-done | bytes 196640 | tf_op jit(solution)/shard_map/ppermute | solution.py:26
  202.3 2.2 collective-permute-done.1
  204.5 0.1 maximum_bitcast_fusion
  204.6 1.5 gather_fusion.1
  206.2 64.4 %all-gather.6.cloned.1.call-done = bf16[32,48,2048]{2,1,0:T(8,128)(2,1)} async-done(((bf16[4,48,2048]{2,1,0:T(8,128)(2,1)}), bf16[32,48,2048]{2,1,0:T(8,128)(2,1)}) %all-gather.6.cloned.1.call-update) | async-done | bytes 6291472 | tf_op jit(solution)/shard_map/all_gather | solution.py:165
  270.6 10.0 %fusion.18 = f32[1536,896]{1,0:T(8,128)S(1)} fusion(bf16[1536,2048]{1,0:T(8,128)(2,1)} %bitcast.115, bf16[1,2048,896]{2,1,0:T(8,128)(2,1)} %param.25), kind=kOutput, calls=%fused_computation.39 | convolution fusion | flops 5637144576 | bytes 15466496 | tf_op jit(solution)/shard_map/dot_general | solution.py:36
  280.6 7.1 %multiply_convert_fusion = bf16[1536,896]{1,0:T(8,128)(2,1)S(1)} fusion(f32[1536,896]{1,0:T(8,128)S(1)} %fusion.18, bf16[1536,2048]{1,0:T(8,128)(2,1)S(1)} %bitcast.116, bf16[1,2048,896]{2,1,0:T(8,128)(2,1)S(1)} %copy-done.7), kind=kOutput, calls=%fused_computation.36 | convolution fusion | flops 5645402112 | bytes 18219008 | tf_op jit(solution)/shard_map/dot_general | solution.py:37
  287.7 8.7 %convert_bitcast_fusion.1 = bf16[32,1,48,2048]{3,2,0,1:T(8,128)(2,1)} fusion(bf16[32,48,896]{2,1,0:T(8,128)(2,1)S(1)} %bitcast.117, bf16[1,896,2048]{2,1,0:T(8,128)(2,1)S(1)} %copy-done.8), kind=kOutput, calls=%fused_computation.35 | convolution fusion | flops 5640290304 | bytes 12713984 | tf_op jit(solution)/shard_map/dot_general | solution.py:39
  296.5 68.5 %reduce-scatter.2.cloned.1.call-done = bf16[4,1,48,2048]{3,2,0,1:T(8,128)(2,1)} async-done(((bf16[32,1,48,2048]{3,2,0,1:T(8,128)(2,1)}), bf16[4,1,48,2048]{3,2,0,1:T(8,128)(2,1)}) %reduce-scatter.2.cloned.1.call-update) | async-done | bytes 786448 | tf_op jit(solution)/shard_map/reduce_scatter | solution.py:175
  365.0 3.8 all-to-all-start.1
  368.8 0.1 copy.91
  368.9 0.1 reshape.248
  369.1 0.1 copy.88
  369.3 8.7 %all-to-all-done.1 = bf16[4,1,48,2048]{3,2,1,0:T(8,128)(2,1)S(1)} async-done(((bf16[4,1,48,2048]{3,2,1,0:T(8,128)(2,1)}), bf16[4,1,48,2048]{3,2,1,0:T(8,128)(2,1)S(1)}, u32[]{:S(2)}, u32[]{:S(2)}) %all-to-all-start.1) | async-done | bytes 786464 | tf_op jit(solution)/shard_map/all_to_all | solution.py:176
  377.9 0.8 gather_fusion.2
  378.8 0.3 reshape.247
  379.0 2.1 multiply_reduce_fusion
  381.1 0.7 add_convert_fusion
  (58 shorter events, 1.1 us)
Async XLA Ops:
  6.5 98.4 %all-gather.4.cloned.1.call-start = ((), (), s32[]{:S(2)}) async-start(), calls=%async_computation.3 | async-start | bytes 9437184 | tf_op jit(solution)/shard_map/all_gather | solution.py:151
  70.6 1.7 copy-start
  88.0 3.0 copy-start.4
  89.6 7.0 %copy-start.3 = (s32[48,2]{0,1:T(2,128)S(1)}, s32[48,2]{0,1:T(2,128)}, u32[]{:S(2)}) copy-start(s32[48,2]{0,1:T(2,128)} %param.28) | copy-start | bytes 1156
  89.8 15.1 %copy-start.1 = (bf16[48,2048]{1,0:T(8,128)(2,1)S(1)}, bf16[48,2048]{1,0:T(8,128)(2,1)}, u32[]{:S(2)}) copy-start(bf16[48,2048]{1,0:T(8,128)(2,1)} %param.23) | copy-start | bytes 589828
  91.8 13.1 %all-to-all-start = ((bf16[8,48,256]{2,1,0:T(8,128)(2,1)}), bf16[8,48,256]{2,1,0:T(8,128)(2,1)S(1)}, u32[]{:S(2)}, u32[]{:S(2)}) async-start(bf16[8,48,256]{2,1,0:T(8,128)(2,1)} %multiply_convert_fusion.2), calls=%async_computation | async-start | bytes 393216 | tf_op jit(solution)/shard_map/all_to_all | solution.py:148
  96.5 174.1 %all-gather.6.cloned.1.call-start = ((), (), s32[]{:S(2)}) async-start(), calls=%async_computation.5 | async-start | bytes 7077888 | tf_op jit(solution)/shard_map/all_gather | solution.py:165
  104.9 5.1 %copy-start.2 = (f32[2048]{0:T(1024)S(1)}, f32[2048]{0:T(1024)}, u32[]{:S(2)}) copy-start(f32[2048]{0:T(1024)} %param.24) | copy-start | bytes 24580
  111.5 90.8 %collective-permute-start = (bf16[1,1,48,2048]{3,2,1,0:T(8,128)(2,1)S(1)}, bf16[1,1,48,2048]{3,2,1,0:T(8,128)(2,1)S(1)}, u32[]{:S(2)}, u32[]{:S(2)}) collective-permute-start(bf16[1,1,48,2048]{3,2,1,0:T(8,128)(2,1)S(1)} %get-tuple-element.272), channel_id=1, source_target_pairs={{0,8},{8,16},{16,24},{24,0},{1,9},{9,17},{17,25},{25,1},{2,10},{10... | collective-permute-start | bytes 589832 | tf_op jit(solution)/shard_map/ppermute | solution.py:26
  139.9 64.6 %collective-permute-start.1 = (bf16[1,1,48,2048]{3,2,1,0:T(8,128)(2,1)S(1)}, bf16[1,1,48,2048]{3,2,1,0:T(8,128)(2,1)S(1)}, u32[]{:S(2)}, u32[]{:S(2)}) collective-permute-start(bf16[1,1,48,2048]{3,2,1,0:T(8,128)(2,1)S(1)} %get-tuple-element.271), channel_id=1, source_target_pairs={{0,16},{8,24},{16,0},{24,8},{1,17},{9,25},{17,1},{25,9},{2,18},{10... | collective-permute-start | bytes 589832 | tf_op jit(solution)/shard_map/ppermute | solution.py:26
  197.0 7.4 %collective-permute-start.2 = (bf16[1,1,48,2048]{3,2,1,0:T(8,128)(2,1)S(1)}, bf16[1,1,48,2048]{3,2,1,0:T(8,128)(2,1)S(1)}, u32[]{:S(2)}, u32[]{:S(2)}) collective-permute-start(bf16[1,1,48,2048]{3,2,1,0:T(8,128)(2,1)S(1)} %get-tuple-element.270), channel_id=1, source_target_pairs={{0,24},{8,0},{16,8},{24,16},{1,25},{9,1},{17,9},{25,17},{2,26},{10... | collective-permute-start | bytes 589832 | tf_op jit(solution)/shard_map/ppermute | solution.py:26
  206.1 158.9 %reduce-scatter.2.cloned.1.call-start = ((), (), s32[]{:S(2)}) async-start(), calls=%async_computation.4 | async-start | bytes 7077888 | tf_op jit(solution)/shard_map/reduce_scatter | solution.py:175
  270.6 10.0 %copy-start.6 = (bf16[32,48,2048]{2,1,0:T(8,128)(2,1)S(1)}, bf16[32,48,2048]{2,1,0:T(8,128)(2,1)}, u32[]{:S(2)}) copy-start(bf16[32,48,2048]{2,1,0:T(8,128)(2,1)} %all-gather.6.cloned.1.call-done) | copy-start | bytes 18874372
  270.6 10.0 %copy-start.7 = (bf16[1,2048,896]{2,1,0:T(8,128)(2,1)S(1)}, bf16[1,2048,896]{2,1,0:T(8,128)(2,1)}, u32[]{:S(2)}) copy-start(bf16[1,2048,896]{2,1,0:T(8,128)(2,1)} %param.26) | copy-start | bytes 11010052
  280.6 7.1 %copy-start.8 = (bf16[1,896,2048]{2,1,0:T(8,128)(2,1)S(1)}, bf16[1,896,2048]{2,1,0:T(8,128)(2,1)}, u32[]{:S(2)}) copy-start(bf16[1,896,2048]{2,1,0:T(8,128)(2,1)} %param.27) | copy-start | bytes 11010052
  296.4 72.7 %copy-start.5 = (f32[48,2]{0,1:T(2,128)S(1)}, f32[48,2]{0,1:T(2,128)}, u32[]{:S(2)}) copy-start(f32[48,2]{0,1:T(2,128)} %param.29) | copy-start | bytes 1156
  365.0 12.9 %all-to-all-start.1 = ((bf16[4,1,48,2048]{3,2,1,0:T(8,128)(2,1)}), bf16[4,1,48,2048]{3,2,1,0:T(8,128)(2,1)S(1)}, u32[]{:S(2)}, u32[]{:S(2)}) async-start(bf16[4,1,48,2048]{3,2,1,0:T(8,128)(2,1)} %bitcast.107), calls=%async_computation.2 | async-start | bytes 1572864 | tf_op jit(solution)/shard_map/all_to_all | solution.py:176
Sparse Core Ops, SparseCore 0:
  8.9 84.7 all-gather.3
  206.2 64.3 all-gather.5
  296.6 68.3 reduce-scatter.1
